TPU v7x, 32 devices: a whole 2x2x4 slice. The times are simulated.
32 devices in a mesh: sp: 8 (over z, y), tp: 4 (over x, core).
Axes of the slice: x: 2, y: 2, z: 4, core: 2. Of those that a mesh axis runs over, the one named last changes fastest.
Arguments:
- skip_stream: bfloat16 [2048, 2048], P('sp', 'tp'), may hold values from -20 to 20
- narrow_lookup_matrix: bfloat16 [2048, 256], P('sp', 'tp'), may hold values from -6 to 6
- narrow_probe_matrix: bfloat16 [2048, 256], P('sp', 'tp'), may hold values from -6 to 6
- narrow_retention_logits: bfloat16 [2048, 256], P('sp', 'tp'), may hold values from -6 to 16
- broad_lookup_matrix: bfloat16 [2048, 512], P('sp', 'tp'), may hold values from -6 to 6
- broad_probe_matrix: bfloat16 [2048, 512], P('sp', 'tp'), may hold values from -6 to 6
- broad_retention_logits: bfloat16 [2048, 512], P('sp', 'tp'), may hold values from -6 to 16
- content_vectors: bfloat16 [2048, 4, 2, 128], P('sp', 'tp'), may hold values from -6 to 6
- extra_log_retention: float32 [2048, 2, 4], P('sp', None, 'tp'), may hold values from -0.7 to 0
- per_branch_scaling: bfloat16 [4, 2, 128], P('tp'), may hold values from 0.099609375 to 1.8984375
- final_projection_matrix: bfloat16 [1024, 2048], P(None, 'tp'), may hold values from -0.1875 to 0.1875
- channel_blend_scaling: bfloat16 [2048], replicated, may hold values from 0.099609375 to 1.8984375
- switch_expansion_matrix: bfloat16 [2048, 5632], P('sp', 'tp'), may hold values from -0.125 to 0.125
- content_expansion_matrix: bfloat16 [2048, 5632], P('sp', 'tp'), may hold values from -0.125 to 0.125
- convolution_kernel: bfloat16 [3, 2, 5632], P(None, None, 'tp'), may hold values from -3.5 to 3.5
- contraction_matrix: bfloat16 [5632, 2048], P('tp', 'sp'), may hold values from -0.078125 to 0.078125
Outputs:
- mixed: bfloat16 [2048, 2048], P('sp', 'tp')
All inputs are finite; a program needn't handle non-finite values.
Results may differ from a plain program's by a relative error of at most 0.011.
Values may be sent and summed in bfloat16 or wider, within the bound.
A program may use at most 64 MiB of HBM per device.

v0:
```python
import jax
import jax.numpy as jnp
from jax import lax
from jax.sharding import PartitionSpec as P

BLOCK = 64


EPSILON = 1e-06
SOFTENING = 16.0
HIGHEST = lax.Precision.HIGHEST


def entering(value, axis, combine, identity):
    devices, mine = (lax.axis_size(axis), lax.axis_index(axis))
    everything = jax.tree.map(
        lambda part, kind: lax.all_gather(part.astype(kind), axis),
        value,
        jax.tree.map(lambda a: jnp.bfloat16 if a.dtype == jnp.float32 else a.dtype, value),
    )
    start = jax.tree.map(
        lambda part, zero: jnp.broadcast_to(jnp.asarray(zero, part.dtype), part.shape),
        value,
        identity,
    )

    def turn(k, before):
        reached = k < mine
        new = combine(
            before, jax.tree.map(lambda part, own: part[k].astype(own.dtype), everything, value)
        )
        return jax.tree.map(lambda a, b: jnp.where(reached, a, b), new, before)

    return lax.fori_loop(0, devices, turn, start)


def shifted(value, axis, steps):
    count = lax.axis_size(axis)
    initial, last = (max(0, -steps), min(count, count - steps))
    return lax.ppermute(value, axis, [(source, source + steps) for source in range(initial, last)])


def blocked(array):
    return array.reshape(array.shape[0] // BLOCK, BLOCK, array.shape[1], array.shape[2]).transpose(
        0, 2, 1, 3
    )


def group_parts(query_rows, input_keys, values_in, log_decay):
    query_blocks = blocked(query_rows)
    key_blocks = blocked(input_keys)
    value_blocks = blocked(values_in)
    inner = jnp.cumsum(blocked(log_decay), axis=2)
    last = inner[:, :, -1:, :]
    middle = inner[:, :, BLOCK // 2 - 1 : BLOCK // 2, :]
    scores = jnp.einsum(
        "nhid,nhjd->nhij",
        query_blocks * jnp.exp(inner - middle),
        key_blocks * jnp.exp(middle - inner),
        precision=HIGHEST,
    )
    lower = jnp.tril(jnp.ones((BLOCK, BLOCK), dtype=bool))
    local_out = jnp.einsum(
        "nhij,nhjv->nhiv", jnp.where(lower, scores, 0.0), value_blocks, precision=HIGHEST
    )
    query_carry = query_blocks * jnp.exp(inner)
    key_carry = key_blocks * jnp.exp(last - inner)
    block_logs = last[:, :, 0, :]
    fade = jnp.exp(block_logs)
    totals = jnp.sum(block_logs, axis=0)
    after = totals[None] - jnp.cumsum(block_logs, axis=0)
    summary = jnp.einsum(
        "nhjd,nhjv->hdv", key_carry * jnp.exp(after)[:, :, None, :], value_blocks, precision=HIGHEST
    )
    return ((local_out, query_carry, key_carry, value_blocks, fade), (jnp.exp(totals), summary))


def group_finish(parts, incoming):
    local_out, query_carry, key_carry, value_blocks, fade = parts

    def advance(state, inputs):
        query_part, key_part, value_part, fade_part = inputs
        output = jnp.einsum("hid,hdv->hiv", query_part, state, precision=HIGHEST)
        state = fade_part[..., None] * state + jnp.einsum(
            "hjd,hjv->hdv", key_part, value_part, precision=HIGHEST
        )
        return (state, output)

    _, carried = lax.scan(advance, incoming, (query_carry, key_carry, value_blocks, fade))
    total = local_out + carried
    return total.transpose(0, 2, 1, 3).reshape(-1, total.shape[1], total.shape[3])


def head_norm(output, gain):
    scale = lax.rsqrt(jnp.mean(output * output, axis=-1, keepdims=True) + EPSILON)
    return output * scale * gain.astype(jnp.float32)


def chain(earlier, later):
    joined = []
    for (fade_early, state_early), (fade_late, state_late) in zip(earlier, later):
        joined.append((fade_early * fade_late, fade_late[..., None] * state_early + state_late))
    return tuple(joined)


def convolve(upward, tap_rows):
    return tap_rows[0] * upward[:-2] + tap_rows[1] * upward[1:-1] + tap_rows[2] * upward[2:]


def local(
    skip_stream,
    narrow_lookup_matrix,
    narrow_probe_matrix,
    narrow_retention_logits,
    broad_lookup_matrix,
    broad_probe_matrix,
    broad_retention_logits,
    content_vectors,
    extra_log_retention,
    per_branch_scaling,
    final_projection_matrix,
    channel_blend_scaling,
    switch_expansion_matrix,
    content_expansion_matrix,
    convolution_kernel,
    contraction_matrix,
):
    item_count = skip_stream.shape[0]
    heads = content_vectors.shape[1]
    value_data = content_vectors.astype(jnp.float32)

    def build_arguments(query_rows, input_keys, forget_gates, spike_column):
        model_width = forget_gates.shape[1] // heads
        query_data = query_rows.astype(jnp.float32).reshape(
            item_count, heads, model_width
        ) * model_width ** (-0.5)
        key_data = input_keys.astype(jnp.float32).reshape(item_count, heads, model_width)
        decay_factor = (
            jax.nn.log_sigmoid(
                forget_gates.astype(jnp.float32).reshape(item_count, heads, model_width)
            )
            / SOFTENING
            + spike_column[:, :, None]
        )
        return (query_data, key_data, decay_factor)

    narrow_lookup_vector, narrow_probe_vector, narrow_probe_dim = build_arguments(
        narrow_lookup_matrix,
        narrow_probe_matrix,
        narrow_retention_logits,
        extra_log_retention[:, 0],
    )
    broad_lookup_vector, broad_probe_vector, broad_probe_dim = build_arguments(
        broad_lookup_matrix, broad_probe_matrix, broad_retention_logits, extra_log_retention[:, 1]
    )
    parts_small, summary_small = group_parts(
        narrow_lookup_vector, narrow_probe_vector, value_data[:, :, 0], narrow_probe_dim
    )
    parts_large, summary_large = group_parts(
        broad_lookup_vector, broad_probe_vector, value_data[:, :, 1], broad_probe_dim
    )
    identity = (
        (jnp.ones_like(summary_small[0]), jnp.zeros_like(summary_small[1])),
        (jnp.ones_like(summary_large[0]), jnp.zeros_like(summary_large[1])),
    )
    incoming = entering((summary_small, summary_large), "sp", chain, identity)
    out_small = group_finish(parts_small, incoming[0][1])
    out_large = group_finish(parts_large, incoming[1][1])
    stacked = jnp.stack(
        [
            head_norm(out_small, per_branch_scaling[:, 0]),
            head_norm(out_large, per_branch_scaling[:, 1]),
        ],
        axis=2,
    )
    heads_in = stacked.reshape(item_count, -1).astype(jnp.bfloat16)
    projected = jnp.dot(
        lax.all_gather(heads_in, "tp", axis=1, tiled=True),
        final_projection_matrix,
        preferred_element_type=jnp.float32,
    )
    resid_data = (
        (skip_stream.astype(jnp.float32) + projected).astype(jnp.bfloat16).astype(jnp.float32)
    )
    resid = resid_data.astype(jnp.bfloat16)
    whole = lax.all_gather(resid, "tp", axis=1, tiled=True).astype(jnp.float32)
    scale = lax.rsqrt(jnp.mean(whole * whole, axis=1, keepdims=True) + EPSILON)
    normed = (whole * scale * channel_blend_scaling.astype(jnp.float32)).astype(jnp.bfloat16)
    gate_rows, value_rows = (
        lax.all_gather(switch_expansion_matrix, "sp", axis=0, tiled=True),
        lax.all_gather(content_expansion_matrix, "sp", axis=0, tiled=True),
    )
    up_gate = jnp.dot(normed, gate_rows, preferred_element_type=jnp.float32).astype(jnp.bfloat16)
    up_value = jnp.dot(normed, value_rows, preferred_element_type=jnp.float32).astype(jnp.bfloat16)
    earlier_rows = shifted((up_value[-2:], up_gate[-2:]), "sp", 1)
    taps = convolution_kernel.astype(jnp.float32)
    value_ext = jnp.concatenate([earlier_rows[0], up_value], axis=0).astype(jnp.float32)
    gate_ext = jnp.concatenate([earlier_rows[1], up_gate], axis=0).astype(jnp.float32)
    conv_value = convolve(value_ext, taps[:, 0])
    conv_gate = convolve(gate_ext, taps[:, 1])
    hidden = (jax.nn.silu(conv_gate) * conv_value).astype(jnp.bfloat16)
    terms = jnp.dot(
        hidden,
        lax.all_gather(contraction_matrix, "sp", axis=1, tiled=True),
        preferred_element_type=jnp.float32,
    )
    down = lax.psum_scatter(
        terms.astype(jnp.bfloat16), "tp", scatter_dimension=1, tiled=True
    ).astype(jnp.float32)
    return (resid_data + down).astype(jnp.bfloat16)


def solution(mesh):
    in_specs = (
        P("sp", "tp"),
        P("sp", "tp"),
        P("sp", "tp"),
        P("sp", "tp"),
        P("sp", "tp"),
        P("sp", "tp"),
        P("sp", "tp"),
        P("sp", "tp", None, None),
        P("sp", None, "tp"),
        P("tp", None, None),
        P(None, "tp"),
        P(),
        P("sp", "tp"),
        P("sp", "tp"),
        P(None, None, "tp"),
        P("tp", "sp"),
    )
    out_specs = P("sp", "tp")
    return jax.shard_map(local, mesh=mesh, in_specs=in_specs, out_specs=out_specs, check_vma=False)
```

profile of v0, /device:TPU:16, one launch (start us, length us, event | category | flops | bytes accessed | tf_op | source)
XLA Modules:
  0.0 463.3 jit_solution(4777201416008957610)
XLA Ops:
  6.6 1.3 fusion.88
  7.9 1.2 fusion.87
  11.3 26.4 %all-gather.3 = bf16[1024,128]{1,0:T(8,128)(2,1)S(1)} all-gather(bf16[128,128]{1,0:T(8,128)(2,1)S(1)} %fusion.42), channel_id=5, replica_groups=mesh['sp'=8,'tp'=4] {'sp'}, dimensions={0}, use_global_device_ids=true | all-gather | bytes 294912 | tf_op jit(solution)/shard_map/all_gather | solution.py:17
  38.5 30.5 %all-gather.1 = bf16[512,128]{1,0:T(8,128)(2,1)S(1)} all-gather(bf16[64,128]{1,0:T(8,128)(2,1)S(1)} %fusion.43), channel_id=3, replica_groups=mesh['sp'=8,'tp'=4] {'sp'}, dimensions={0}, use_global_device_ids=true | all-gather | bytes 147456 | tf_op jit(solution)/shard_map/all_gather | solution.py:17
  70.4 20.5 %all-reduce = bf16[512]{0:T(512)(128)(2,1)S(1)} all-reduce(bf16[512]{0:T(512)(128)(2,1)S(1)} %dynamic-update-slice), channel_id=2, replica_groups=mesh['sp'=8,'tp'=4] {'sp'}, use_global_device_ids=true, to_apply=%add | all-reduce | flops 512 | bytes 2048
  91.0 16.9 %all-gather.4 = bf16[8,1,128]{2,1,0:T(2,128)(2,1)S(1)} all-gather(bf16[1,1,128]{2,1,0:T(2,128)(2,1)S(1)} %convert_bitcast_fusion), channel_id=4, replica_groups=mesh['sp'=8,'tp'=4] {'sp'}, dimensions={0}, use_global_device_ids=true | all-gather | bytes 2304 | tf_op jit(solution)/shard_map/all_gather | solution.py:17
  107.9 1.6 while.42
  109.8 1.8 while.40
  112.6 2.1 while.41
  115.8 7.2 %all_gather.41 = bf16[256,1024]{0,1:T(8,128)(2,1)S(1)} all-gather(bf16[256,256]{0,1:T(8,128)(2,1)S(1)} %bitcast.236), channel_id=1, replica_groups=mesh['sp'=8,'tp'=4] {'tp'}, dimensions={1}, use_global_device_ids=true | all-gather | bytes 655360 | tf_op jit(solution)/shard_map/all_gather | solution.py:178
  126.4 17.4 %all-gather.10.cloned.1.call-done = bf16[256,2048]{1,0:T(8,128)(2,1)} async-done(((bf16[256,512]{1,0:T(8,128)(2,1)}), bf16[256,2048]{1,0:T(8,128)(2,1)}) %all-gather.10.cloned.1.call-update) | async-done | bytes 1048592 | tf_op jit(solution)/shard_map/all_gather | solution.py:186
  143.8 1.5 fusion.30
  145.4 92.1 %all-gather.12.cloned.1.call-done = bf16[2048,1408]{1,0:T(8,128)(2,1)} async-done(((bf16[256,1408]{1,0:T(8,128)(2,1)}), bf16[2048,1408]{1,0:T(8,128)(2,1)}) %all-gather.12.cloned.1.call-update) | async-done | bytes 5767184 | tf_op jit(solution)/shard_map/all_gather | solution.py:190
  237.5 4.8 %convolution_convert_fusion.1 = bf16[256,1408]{1,0:T(8,128)(2,1)S(1)} fusion(bf16[2048,1408]{1,0:T(8,128)(2,1)} %all-gather.12.cloned.1.call-done, bf16[256,2048]{1,0:T(8,128)(2,1)} %all-gather.10.cloned.1.call-done, f32[2048]{0:T(1024)S(1)} %convert_element_type.216, f32[256]{0:T(256)S(1)} %add_rsqrt_fusion.2), kind=kOutput, calls=%fused_computation.43 | convolution fusion | flops 1478852608 | bytes 7545856 | tf_op jit(solution)/shard_map/dot_general | solution.py:193
  243.2 2.5 collective-permute-start
  245.6 84.5 %all-gather.14.cloned.1.call-done = bf16[2048,1408]{1,0:T(8,128)(2,1)} async-done(((bf16[256,1408]{1,0:T(8,128)(2,1)}), bf16[2048,1408]{1,0:T(8,128)(2,1)}) %all-gather.14.cloned.1.call-update) | async-done | bytes 5767184 | tf_op jit(solution)/shard_map/all_gather | solution.py:191
  330.2 4.6 convolution_convert_fusion
  334.8 2.5 collective-permute-start.1
  337.4 3.8 collective-permute-done.1
  341.2 1.3 maximum_convert_fusion.1
  342.5 81.0 %all-gather.16.cloned.1.call-done = bf16[1408,2048]{1,0:T(8,128)(2,1)} async-done(((bf16[1408,256]{1,0:T(8,128)(2,1)}), bf16[1408,2048]{1,0:T(8,128)(2,1)}) %all-gather.16.cloned.1.call-update) | async-done | bytes 5767184 | tf_op jit(solution)/shard_map/all_gather | solution.py:204
  423.4 7.6 %convolution_convert_fusion.2 = bf16[256,2048]{1,0:T(8,128)(2,1)} fusion(bf16[1408,2048]{1,0:T(8,128)(2,1)} %all-gather.16.cloned.1.call-done, f32[258,1408]{1,0:T(8,128)} %maximum_convert_fusion.1, f32[258,1408]{1,0:T(8,128)S(1)} %maximum_convert_fusion, f32[1408]{0:T(1024)S(1)} %get-tuple-element.317, f32[1408]{0:T(1024)S(1)} %get-tuple-element.318, ...), kind=kOutput, calls=%fused_computation.44 | convolution fusion | flops 1482686464 | bytes 15515648 | tf_op jit(solution)/shard_map/dot_general | solution.py:202
  431.1 24.0 %reduce-scatter.2.cloned.1.call-done = bf16[256,512]{1,0:T(8,128)(2,1)} async-done(((bf16[256,2048]{1,0:T(8,128)(2,1)}), bf16[256,512]{1,0:T(8,128)(2,1)}) %reduce-scatter.2.cloned.1.call-update) | async-done | bytes 262160 | tf_op jit(solution)/shard_map/reduce_scatter | solution.py:207
  455.1 1.7 add_convert_fusion
  (152 shorter events, 15.6 us)
Async XLA Ops:
  6.5 116.4 %copy-start = (bf16[1024,512]{1,0:T(8,128)(2,1)S(1)}, bf16[1024,512]{1,0:T(8,128)(2,1)}, u32[]{:S(2)}) copy-start(bf16[1024,512]{1,0:T(8,128)(2,1)} %param.32) | copy-start | bytes 3145732
  6.5 4.5 copy-start.5
  6.5 31.2 %copy-start.7 = (bf16[256,64]{0,1:T(8,128)(2,1)S(1)}, bf16[256,64]{0,1:T(8,128)(2,1)}, u32[]{:S(2)}) copy-start(bf16[256,64]{0,1:T(8,128)(2,1)} %param.25) | copy-start | bytes 98308
  6.5 137.3 %all-gather.10.cloned.1.call-start = ((), (), s32[]{:S(2)}) async-start(), calls=%async_computation.1 | async-start | bytes 1310720 | tf_op jit(solution)/shard_map/all_gather | solution.py:186
  7.9 30.2 %copy-start.8 = (bf16[256,64]{0,1:T(8,128)(2,1)S(1)}, bf16[256,64]{0,1:T(8,128)(2,1)}, u32[]{:S(2)}) copy-start(bf16[256,64]{0,1:T(8,128)(2,1)} %param.24) | copy-start | bytes 98308
  9.8 59.2 %copy-start.14 = (u32[32]{0:T(128)S(1)}, u32[32]{0:T(128)}, u32[]{:S(2)}) copy-start(u32[32]{0:T(128)} %constant.109) | copy-start | bytes 388
  37.7 71.9 %copy-start.9 = (bf16[256,64]{0,1:T(8,128)(2,1)S(1)}, bf16[256,64]{0,1:T(8,128)(2,1)}, u32[]{:S(2)}) copy-start(bf16[256,64]{0,1:T(8,128)(2,1)} %param.23) | copy-start | bytes 98308
  109.8 2.7 copy-start.6
  112.6 3.1 copy-start.12
  114.7 8.2 %copy-start.13 = (bf16[256,512]{1,0:T(8,128)(2,1)S(1)}, bf16[256,512]{1,0:T(8,128)(2,1)}, u32[]{:S(2)}) copy-start(bf16[256,512]{1,0:T(8,128)(2,1)} %param.22) | copy-start | bytes 786436
  124.1 2.1 copy-start.11
  124.1 2.2 copy-start.10
  124.1 113.3 %all-gather.12.cloned.1.call-start = ((), (), s32[]{:S(2)}) async-start(), calls=%async_computation.2 | async-start | bytes 6488064 | tf_op jit(solution)/shard_map/all_gather | solution.py:190
  124.9 205.3 %all-gather.14.cloned.1.call-start = ((), (), s32[]{:S(2)}) async-start(), calls=%async_computation.3 | async-start | bytes 6488064 | tf_op jit(solution)/shard_map/all_gather | solution.py:191
  125.6 297.8 %all-gather.16.cloned.1.call-start = ((), (), s32[]{:S(2)}) async-start(), calls=%async_computation.4 | async-start | bytes 6488064 | tf_op jit(solution)/shard_map/all_gather | solution.py:204
  126.2 328.9 %reduce-scatter.2.cloned.1.call-start = ((), (), s32[]{:S(2)}) async-start(), calls=%async_computation.5 | async-start | bytes 1310720 | tf_op jit(solution)/shard_map/reduce_scatter | solution.py:207
  145.3 184.8 %copy-start.2 = (bf16[256,2048]{1,0:T(8,128)(2,1)S(1)}, bf16[256,2048]{1,0:T(8,128)(2,1)}, u32[]{:S(2)}) copy-start(bf16[256,2048]{1,0:T(8,128)(2,1)} %all-gather.10.cloned.1.call-done) | copy-start | bytes 3145732
  242.3 0.9 copy-start.3
  243.2 94.1 %collective-permute-start = (bf16[2,1408]{1,0:T(2,128)(2,1)S(1)}, bf16[2,1408]{1,0:T(2,128)(2,1)S(1)}, u32[]{:S(2)}, u32[]{:S(2)}) collective-permute-start(bf16[2,1408]{1,0:T(2,128)(2,1)S(1)} %slice.123), channel_id=1, source_target_pairs={{0,4},{4,8},{8,12},{12,16},{16,20},{20,24},{24,28},{1,5},{5,9},{9,... | collective-permute-start | bytes 16904 | tf_op jit(solution)/shard_map/ppermute | solution.py:40
  330.2 7.1 %copy-start.4 = (bf16[256,1408]{1,0:T(8,128)(2,1)S(1)}, bf16[256,1408]{1,0:T(8,128)(2,1)}, u32[]{:S(2)}) copy-start(bf16[256,1408]{1,0:T(8,128)(2,1)} %copy-done.3) | copy-start | bytes 2162692
  334.8 6.4 %collective-permute-start.1 = (bf16[2,1408]{1,0:T(2,128)(2,1)S(1)}, bf16[2,1408]{1,0:T(2,128)(2,1)S(1)}, u32[]{:S(2)}, u32[]{:S(2)}) collective-permute-start(bf16[2,1408]{1,0:T(2,128)(2,1)S(1)} %slice.130), channel_id=1, source_target_pairs={{0,4},{4,8},{8,12},{12,16},{16,20},{20,24},{24,28},{1,5},{5,9},{9,... | collective-permute-start | bytes 16904 | tf_op jit(solution)/shard_map/ppermute | solution.py:40
  423.4 31.7 %copy-start.1 = (bf16[256,512]{1,0:T(8,128)(2,1)S(1)}, bf16[256,512]{1,0:T(8,128)(2,1)}, u32[]{:S(2)}) copy-start(bf16[256,512]{1,0:T(8,128)(2,1)} %fusion.39) | copy-start | bytes 786436
Sparse Core Ops, SparseCore 0:
  124.3 19.5 all-gather.9
  146.0 91.4 all-gather.11
  239.6 90.4 all-gather.13
  332.1 91.3 all-gather.15
  431.2 23.8 reduce-scatter.1
where the time goes:
time: 465 us; the launch traced here: 463 us
  waiting for transfers between devices  305 us (66%)
  blocking collectives  101 us (22%)
  matrix products  23.7 us (5%)
  between operations  14.1 us (3%)
  other arithmetic  7.93 us (2%)
  local copies, waits for them, and re-layouts  5.9 us (1%)
  starting transfers between devices  5.07 us (1%)
    all_gather x1, waiting for transfers between devices, local(): lax.all_gather(switch_expansion_matrix, 'sp', axis=0, tiled=True)  92.1 us
    all_gather x1, waiting for transfers between devices, local(): lax.all_gather(content_expansion_matrix, 'sp', axis=0, tiled=True)  84.5 us
    all_gather x1, waiting for transfers between devices, local(): lax.all_gather(contraction_matrix, 'sp', axis=1, tiled=True)  81 us
    all_gather x3, blocking collectives, entering(): lax.all_gather(part.astype(kind), axis)  73.8 us
    reduce_scatter x1, waiting for transfers between devices, local(): lax.psum_scatter(terms.astype(jnp.bfloat16), 'tp', scatter_dimension=1, t...  24 us
    unnamed x1, blocking collectives  20.5 us
    all_gather x1, waiting for transfers between devices, local(): whole = lax.all_gather(resid, 'tp', axis=1, tiled=True).astype(jnp.float32)  17.4 us
  transfers between devices with their start and end apart: 7, of which 6 were waited for; matrix products, arithmetic and copies ran while one was open for 3% of the time, Pallas kernels for 0%

commit v1 on v0

v1 whole, which is shorter than its diff:
```python
import functools

import jax
import jax.numpy as jnp
from jax import lax
from jax.experimental import pallas as pl
from jax.experimental.pallas import tpu as pltpu
from jax.sharding import PartitionSpec as P

BLOCK = 64
HALO = 16
EPSILON = 1e-06
SOFTENING = 16.0
HIGHEST = lax.Precision.HIGHEST
F32 = jnp.float32
BF16 = jnp.bfloat16
NT = (((1,), (1,)), ((), ()))


def blocked(array):
    return array.reshape(array.shape[0] // BLOCK, BLOCK, array.shape[1], array.shape[2]).transpose(
        0, 2, 1, 3
    )


def local_attention(q, k, v, log_decay):
    tokens, units, key = q.shape
    query_blocks, key_blocks, value_blocks = blocked(q), blocked(k), blocked(v)
    lower = jnp.tril(jnp.ones((BLOCK, BLOCK), dtype=bool))
    inner = jnp.einsum(
        "ij,nhjd->nhid", lower.astype(F32), blocked(log_decay), precision=HIGHEST
    )
    last = inner[:, :, -1:, :]
    middle = inner[:, :, BLOCK // 2 - 1 : BLOCK // 2, :]
    scores = jnp.einsum(
        "nhid,nhjd->nhij",
        query_blocks * jnp.exp(inner - middle),
        key_blocks * jnp.exp(middle - inner),
        precision=HIGHEST,
    )
    out = jnp.einsum(
        "nhij,nhjv->nhiv", jnp.where(lower, scores, 0.0), value_blocks, precision=HIGHEST
    )
    query_carry = query_blocks * jnp.exp(inner)
    key_carry = key_blocks * jnp.exp(last - inner)
    added = jnp.einsum("nhjd,nhjv->nhvd", key_carry, value_blocks, precision=HIGHEST)
    block_logs = last[:, :, 0, :]
    before = jnp.cumsum(block_logs, axis=0) - block_logs
    state, states = jnp.zeros_like(added[0]), []
    for n in range(added.shape[0]):
        states.append(state)
        state = jnp.exp(block_logs[n])[:, None, :] * state + added[n]
    out = out + jnp.einsum("nhid,nhvd->nhiv", query_carry, jnp.stack(states), precision=HIGHEST)
    meets = query_carry * jnp.exp(before)[:, :, None, :]
    fade = jnp.exp(jnp.sum(block_logs, axis=0))

    def unblock(a):
        return a.transpose(0, 2, 1, 3).reshape(tokens, -1)

    return unblock(out), unblock(meets), state, fade


def kernel(
    n_sp, n_tp, units,
    w_ref, st_ref, out_ref0, meets_ref, gain_ref, skip_ref, proj_ref, blend_ref, taps_ref,
    mixed_ref,
    wbuf, stbuf, acc_state, heads, resid, nb, up, hid, psum, rbuf,
    own_sem, st_send, st_recv, uz_send, uz_recv, uy_send, uy_recv, cz_send, cz_recv, cy_send,
    cy_recv, h_send, h_recv, r_send, r_recv, n_send, n_recv, d_send, d_recv,
):
    s, t = lax.axis_index("sp"), lax.axis_index("tp")
    nz = n_sp // 2
    z, y = s // 2, s % 2
    q = z % 2
    mate = s + 2 - 4 * q
    side = s + 1 - 2 * y
    tok = skip_ref.shape[0]
    cols = skip_ref.shape[1]
    half = wbuf.shape[2]
    dblk = wbuf.shape[3]
    dv = out_ref0.shape[1] // units

    def rc(src, dst, ss, rs, sp, tp):
        return pltpu.make_async_remote_copy(
            src_ref=src, dst_ref=dst, send_sem=ss, recv_sem=rs,
            device_id=(sp, tp), device_id_type=pl.DeviceIdType.MESH,
        )

    bar = pltpu.get_barrier_semaphore()
    count = 0
    for o in range(1, n_sp):
        pl.semaphore_signal(bar, inc=1, device_id=(lax.rem(s + o, n_sp), t),
                            device_id_type=pl.DeviceIdType.MESH)
        count += 1
    for row in (s, mate):
        for o in range(1, n_tp):
            pl.semaphore_signal(bar, inc=1, device_id=(row, lax.rem(t + o, n_tp)),
                                device_id_type=pl.DeviceIdType.MESH)
            count += 1
    pl.semaphore_wait(bar, count)

    st = [None] + [
        rc(st_ref, stbuf.at[s], st_send.at[o], st_recv.at[o], lax.rem(s + o, n_sp), t)
        for o in range(1, n_sp)
    ]
    for o in range(1, n_sp):
        @pl.when(s + o < n_sp)
        def _(o=o):
            st[o].start()

    def zcopies(lo, width, ss, rs):
        made = []
        for o in range(1, nz):
            zz = lax.rem(z + o, nz)
            rows = pl.ds(pl.multiple_of((zz % 2) * half, HALO), half)
            made.append(rc(w_ref.at[pl.ds(lo, width), rows], wbuf.at[s, pl.ds(lo, width)],
                           ss.at[o], rs.at[o], zz * 2 + y, t))
        return made

    def ycopy(o, lo, width, ss, rs):
        if o == 0:
            rows = pl.ds(pl.multiple_of(q * half, HALO), half)
            source = w_ref.at[pl.ds(lo, width), rows]
            slot = s
        else:
            slot = lax.rem(z + nz - o, nz) * 2 + y
            source = wbuf.at[slot, pl.ds(lo, width)]
        return rc(source, wbuf.at[slot, pl.ds(lo, width)], ss.at[o], rs.at[o], side, t)

    uz = zcopies(0, 2, uz_send, uz_recv)
    uy = [ycopy(o, 0, 2, uy_send, uy_recv) for o in range(nz)]
    for copy in uz:
        copy.start()
    uy[0].start()
    own = pltpu.make_async_copy(
        w_ref.at[:, pl.ds(pl.multiple_of(q * half, HALO), half)], wbuf.at[s], own_sem
    )
    own.start()

    acc_state[...] = jnp.zeros_like(acc_state)
    for o in range(n_sp - 1, 0, -1):
        @pl.when(s - o >= 0)
        def _(o=o):
            st[o].wait_recv()
            got = stbuf[s - o].astype(F32)
            acc_state[...] = got[dv : dv + 1] * acc_state[...] + got[:dv]
    key = meets_ref.shape[1] // units
    mine = []
    for u in range(units):
        total = out_ref0[:, u * dv : (u + 1) * dv] + lax.dot_general(
            meets_ref[:, u * key : (u + 1) * key], acc_state[:, u * key : (u + 1) * key],
            NT, precision=HIGHEST, preferred_element_type=F32,
        )
        scale = lax.rsqrt(jnp.mean(total * total, axis=-1, keepdims=True) + EPSILON)
        mine.append((total * scale * gain_ref[u : u + 1, :]).astype(BF16))
    heads[t] = jnp.concatenate(mine, axis=1)
    hc = [
        rc(heads.at[t], heads.at[t], h_send.at[o], h_recv.at[o], s, lax.rem(t + o, n_tp))
        for o in range(1, n_tp)
    ]
    for copy in hc:
        copy.start()
    for copy in hc:
        copy.wait_recv()
    width = units * dv
    projected = skip_ref[...].astype(F32)
    whole_heads = jnp.concatenate([heads[i] for i in range(n_tp)], axis=1)
    projected = projected + jnp.dot(whole_heads, proj_ref[...], preferred_element_type=F32)
    resid[t] = projected.astype(BF16)
    qc = [
        rc(resid.at[t], resid.at[t], r_send.at[o], r_recv.at[o], s, lax.rem(t + o, n_tp))
        for o in range(1, n_tp)
    ]
    for copy in qc:
        copy.start()
    for copy in qc:
        copy.wait_recv()
    squares = jnp.zeros((tok, 1), F32)
    for i in range(n_tp):
        part = resid[i].astype(F32)
        squares = squares + jnp.sum(part * part, axis=1, keepdims=True)
    scale = lax.rsqrt(squares / (n_tp * cols) + EPSILON)
    for i in range(n_tp):
        piece = slice(i * cols, (i + 1) * cols)
        nb[0, HALO:, piece] = (
            resid[i].astype(F32) * scale * blend_ref[:, piece]
        ).astype(BF16)
    after = lax.rem(s + 1, n_sp)
    after_mate = after + 2 - 4 * ((after // 2) % 2)
    block = pl.ds(HALO, tok)
    tail = pl.ds(tok, HALO)
    nc = [
        rc(nb.at[0, tail], nb.at[0, pl.ds(0, HALO)], n_send.at[0], n_recv.at[0], after, t),
        rc(nb.at[0, tail], nb.at[1, pl.ds(0, HALO)], n_send.at[1], n_recv.at[1], after_mate, t),
        rc(nb.at[0, block], nb.at[1, block], n_send.at[2], n_recv.at[2], mate, t),
    ]
    for copy in nc:
        copy.start()
    cz = zcopies(2, 1, cz_send, cz_recv)
    cy = [ycopy(o, 2, 1, cy_send, cy_recv) for o in range(nz)]
    for copy in cz:
        copy.start()
    for o in range(1, nz):
        uz[o - 1].wait_recv()
        uy[o].start()
    cy[0].start()
    for copy in nc:
        copy.wait_recv()
    own.wait()
    for o in range(nz):
        uy[o].wait_recv()

    for m in range(2):
        for i in range(2):
            up[m, i] = jnp.zeros_like(up[m, i])

    group = max(1, 128 // dblk)

    def expand_add(b, carry):
        at = pl.ds(pl.multiple_of(b * group * dblk, 128), group * dblk)
        for i in range(2):
            rows = nb[i, :, at]
            for j in range(group):
                part = rows[:, j * dblk : (j + 1) * dblk]
                for m in range(2):
                    up[m, i] += lax.dot_general(
                        part, wbuf[b * group + j, m], NT, preferred_element_type=F32
                    )
        return carry

    lax.fori_loop(0, n_sp // group, expand_add, 0)
    for o in range(1, nz):
        cz[o - 1].wait_recv()
        cy[o].start()
    for i in range(2):
        first = (s if i == 0 else mate) == 0
        conv = []
        for m in range(2):
            keep = jnp.where(first, 0.0, 1.0)
            edge = up[m, i, :HALO].astype(BF16).astype(F32)
            up[m, i, :HALO] = edge * keep
            up[m, i, HALO:] = up[m, i, HALO:].astype(BF16).astype(F32)
            total = taps_ref[m * 3 : m * 3 + 1] * up[m, i, pl.ds(HALO - 2, tok)]
            total += taps_ref[m * 3 + 1 : m * 3 + 2] * up[m, i, pl.ds(HALO - 1, tok)]
            total += taps_ref[m * 3 + 2 : m * 3 + 3] * up[m, i, pl.ds(HALO, tok)]
            conv.append(total)
        value, gate = conv
        hid[pl.ds(i * tok, tok)] = (gate / (1.0 + jnp.exp(-gate)) * value).astype(BF16)
    for o in range(nz):
        cy[o].wait_recv()
    per = cols // dblk
    dc = []
    for o in range(1, n_tp + 1):
        to = lax.rem(t + o, n_tp)
        for j in range(per):
            part = jnp.dot(hid[...], wbuf[to * per + j, 2], preferred_element_type=F32).astype(BF16)
            psum[to, 0, :, j * dblk : (j + 1) * dblk] = part[:tok]
            psum[to, 1, :, j * dblk : (j + 1) * dblk] = part[tok:]
        for i in range(2):
            if i == 0 and o == n_tp:
                continue
            at = i * n_tp + o - 1
            copy = rc(psum.at[to, i], rbuf.at[at], d_send.at[at], d_recv.at[at],
                      s if i == 0 else mate, to)
            copy.start()
            dc.append((at, copy))
    total = psum[t, 0].astype(F32)
    for at, copy in dc:
        copy.wait_recv()
        total = total + rbuf[at].astype(F32)
    mixed_ref[...] = (resid[t].astype(F32) + total).astype(BF16)

    for o in range(1, n_sp):
        @pl.when(s + o < n_sp)
        def _(o=o):
            st[o].wait_send()
    for copy in uz + uy + cz + cy + hc + qc + nc + [c for _, c in dc]:
        copy.wait_send()


def local(
    n_sp, n_tp,
    skip_stream,
    narrow_lookup_matrix,
    narrow_probe_matrix,
    narrow_retention_logits,
    broad_lookup_matrix,
    broad_probe_matrix,
    broad_retention_logits,
    content_vectors,
    extra_log_retention,
    per_branch_scaling,
    final_projection_matrix,
    channel_blend_scaling,
    switch_expansion_matrix,
    content_expansion_matrix,
    convolution_kernel,
    contraction_matrix,
):
    tok, cols = skip_stream.shape
    heads = content_vectors.shape[1]
    dv = content_vectors.shape[3]
    narrow = narrow_lookup_matrix.shape[1] // heads
    broad = broad_lookup_matrix.shape[1] // heads
    units = 2 * heads

    def pair(a, b):
        a = a.astype(F32).reshape(tok, heads, narrow)
        b = b.astype(F32).reshape(tok, heads, broad)
        return a, b

    def join(a, b):
        a = jnp.pad(a, ((0, 0), (0, 0), (0, broad - narrow)))
        return jnp.stack([a, b], axis=2).reshape(tok, units, broad)

    qa, qb = pair(narrow_lookup_matrix, broad_lookup_matrix)
    query = join(qa * narrow ** (-0.5), qb * broad ** (-0.5))
    keys = join(*pair(narrow_probe_matrix, broad_probe_matrix))
    gates = join(*pair(narrow_retention_logits, broad_retention_logits))
    extra = extra_log_retention.transpose(0, 2, 1).reshape(tok, units, 1)
    decay = jax.nn.log_sigmoid(gates) / SOFTENING + extra
    values = content_vectors.astype(F32).reshape(tok, units, dv)
    out, meets, state, fade = local_attention(query, keys, values, decay)
    packed = jnp.concatenate(
        [
            state.transpose(1, 0, 2).reshape(dv, units * broad),
            fade.reshape(1, units * broad),
            jnp.zeros((15, units * broad), F32),
        ],
        axis=0,
    ).astype(BF16)
    weights = jnp.stack(
        [content_expansion_matrix.T, switch_expansion_matrix.T, contraction_matrix], axis=0
    )
    ff = contraction_matrix.shape[0]
    half = ff // 2
    dblk = contraction_matrix.shape[1]
    q = (lax.axis_index("sp") // 2) % 2
    taps = lax.dynamic_slice_in_dim(convolution_kernel, q * half, half, axis=2)
    taps = jnp.pad(taps.astype(F32).transpose(1, 0, 2).reshape(6, half), ((0, 2), (0, 0)))
    gain = per_branch_scaling.astype(F32).reshape(units, dv)
    blend = channel_blend_scaling.astype(F32).reshape(1, -1)
    nz = n_sp // 2
    model = n_tp * cols
    dma = pltpu.SemaphoreType.DMA
    vmem = pl.BlockSpec(memory_space=pltpu.VMEM)
    return pl.pallas_call(
        functools.partial(kernel, n_sp, n_tp, units),
        out_shape=jax.ShapeDtypeStruct((tok, cols), BF16),
        in_specs=[vmem] * 9,
        out_specs=vmem,
        scratch_shapes=[
            pltpu.VMEM((n_sp, 3, half, dblk), BF16),
            pltpu.VMEM((n_sp,) + packed.shape, BF16),
            pltpu.VMEM((dv, units * broad), F32),
            pltpu.VMEM((n_tp, tok, units * dv), BF16),
            pltpu.VMEM((n_tp, tok, cols), BF16),
            pltpu.VMEM((2, tok + HALO, model), BF16),
            pltpu.VMEM((2, 2, tok + HALO, half), F32),
            pltpu.VMEM((2 * tok, half), BF16),
            pltpu.VMEM((n_tp, 2, tok, cols), BF16),
            pltpu.VMEM((2 * n_tp, tok, cols), BF16),
            dma,
            dma((n_sp,)), dma((n_sp,)),
            dma((nz,)), dma((nz,)), dma((nz,)), dma((nz,)),
            dma((nz,)), dma((nz,)), dma((nz,)), dma((nz,)),
            dma((n_tp,)), dma((n_tp,)), dma((n_tp,)), dma((n_tp,)),
            dma((3,)), dma((3,)), dma((2 * n_tp,)), dma((2 * n_tp,)),
        ],
        compiler_params=pltpu.CompilerParams(
            collective_id=0, has_side_effects=True, vmem_limit_bytes=56 * 1024 * 1024
        ),
    )(weights, packed, out, meets, gain, skip_stream, final_projection_matrix, blend, taps)


def solution(mesh):
    in_specs = (
        P("sp", "tp"),
        P("sp", "tp"),
        P("sp", "tp"),
        P("sp", "tp"),
        P("sp", "tp"),
        P("sp", "tp"),
        P("sp", "tp"),
        P("sp", "tp", None, None),
        P("sp", None, "tp"),
        P("tp", None, None),
        P(None, "tp"),
        P(),
        P("sp", "tp"),
        P("sp", "tp"),
        P(None, None, "tp"),
        P("tp", "sp"),
    )
    out_specs = P("sp", "tp")
    body = functools.partial(local, mesh.shape["sp"], mesh.shape["tp"])
    return jax.shard_map(body, mesh=mesh, in_specs=in_specs, out_specs=out_specs, check_vma=False)
```

time: 465 us -> 184 us (0.40)
  waiting for transfers between devices: 305 us -> 0 us
  Pallas kernels: 0 us -> 170 us
  blocking collectives: 101 us -> 0 us
  matrix products: 23.7 us -> 2.54 us
  between operations: 14.1 us -> 0.32 us
  starting transfers between devices: 5.07 us -> 0 us
    all_gather x4 -> x0, waiting for transfers between devices: 275 us -> none  [the longest x1 92.1 us: local(): lax.all_gather(switch_expansion_matrix, 'sp', axis=0, tiled=True)]
    pallas_call x0 -> x1, Pallas kernels: none -> 170 us  [local(): pl.pallas_call(functools.partial(kernel, n_sp, n_tp, units), out_shape=ja...]
    all_gather x4 -> x0, blocking collectives: 81 us -> none  [the longest x3 73.8 us: entering(): lax.all_gather(part.astype(kind), axis)]
    reduce_scatter x1 -> x0, waiting for transfers between devices: 24 us -> none  [local(): lax.psum_scatter(terms.astype(jnp.bfloat16), 'tp', scatter_dimension=1, t...]
    dot_general x26 -> x5, matrix products: 23.7 us -> 2.54 us  [the longest x1 0.63 us: local_attention(): jnp.einsum('nhid,nhvd->nhiv', query_carry, jnp.stack(states), precision=H...]
    unnamed x1 -> x0, blocking collectives: 20.5 us -> none
    ppermute x2 -> x0, starting transfers between devices: 4.91 us -> none  [shifted(): lax.ppermute(value, axis, [(source, source + steps) for source in range(i...]
  transfers between devices with their start and end apart: 7 -> 0, of which waited for: 6 -> 0; matrix products, arithmetic and copies ran while one was open for 3% -> 0% of each run, Pallas kernels for 0% -> 0%
where the time goes in v1:
time: 184 us
  Pallas kernels  170 us (92%)
  local copies, waits for them, and re-layouts  6.56 us (4%)
  other arithmetic  4.6 us (2%)
  matrix products  2.54 us (1%)
    pallas_call x1, Pallas kernels, local(): pl.pallas_call(functools.partial(kernel, n_sp, n_tp, units), out_shape=ja...  170 us
    unnamed x31, local copies, waits for them, and re-layouts  4.89 us

profile of v1, /device:TPU:16, one launch (start us, length us, event | category | flops | bytes accessed | tf_op | source)
XLA Modules:
  0.0 183.5 jit_solution(9016748321535564982)
XLA Ops:
  0.0 1.4 copy.31
  1.5 1.4 copy.30
  2.9 1.6 pad_maximum_fusion.w_ref
  4.5 0.1 copy.32
  4.7 0.1 add.65
  4.8 0.4 fusion.14
  5.3 0.1 copy.45
  5.5 0.6 convolution_bitcast_fusion
  6.1 0.2 fusion.24
  6.3 0.1 copy.44
  6.5 0.7 maximum_maximum_fusion.st_ref
  7.3 0.1 copy.46
  7.5 0.2 copy.40
  7.7 0.6 convolution_select_fusion
  8.3 0.3 fusion.28
  8.6 0.2 multiply_add_fusion
  8.8 0.6 fusion
  9.4 0.2 copy.39
  9.6 0.8 copy_bitcast_fusion
  10.5 0.5 bitcast_convert_fusion.gain_ref
  11.0 0.6 reshape.120
  11.7 0.6 pad_convert_fusion.taps_ref
  12.3 169.5 %shard_map.154 = bf16[256,512]{1,0:T(8,128)(2,1)} custom-call(bf16[3,1408,256]{2,1,0:T(8,128)(2,1)} %pad_maximum_fusion.w_ref, bf16[144,256]{1,0:T(8,128)(2,1)} %maximum_maximum_fusion.st_ref, f32[256,256]{1,0:T(8,128)} %get-tuple-element.16.out_ref0, f32[256,256]{1,0:T(8,128)} %get-tuple-element.15.meets_ref, f32[2,128]{1,0:T(2,128)} %bitcast_convert_fusion.gain_ref, ...), custom_call_target="tpu_custom_call" | custom-call | tf_op jit(solution)/shard_map/pallas_call | solution.py:347
  181.9 1.7 copy.65
  (43 shorter events, 0.5 us)
Async XLA Ops:
  0.0 11.6 %copy-start = (bf16[3,2,1408]{2,1,0:T(2,128)(2,1)S(1)}, bf16[3,2,1408]{2,1,0:T(2,128)(2,1)}, u32[]{:S(2)}) copy-start(bf16[3,2,1408]{2,1,0:T(2,128)(2,1)} %param.30) | copy-start | bytes 50692
  0.0 2.8 %copy-start.1 = (bf16[1408,256]{1,0:T(8,128)(2,1)S(1)}, bf16[1408,256]{1,0:T(8,128)(2,1)}, u32[]{:S(2)}) copy-start(bf16[1408,256]{1,0:T(8,128)(2,1)} %param.31) | copy-start | bytes 2162692
  2.9 1.7 copy-start.5
  2.9 1.8 copy-start.9
  2.9 1.9 %copy-start.10 = (bf16[256,128]{1,0:T(8,128)(2,1)S(1)}, bf16[256,128]{1,0:T(8,128)(2,1)}, u32[]{:S(2)}) copy-start(bf16[256,128]{1,0:T(8,128)(2,1)} %param.22) | copy-start | bytes 196612
  2.9 2.4 %copy-start.6 = (bf16[256,64]{0,1:T(8,128)(2,1)S(1)}, bf16[256,64]{0,1:T(8,128)(2,1)}, u32[]{:S(2)}) copy-start(bf16[256,64]{0,1:T(8,128)(2,1)} %param.18) | copy-start | bytes 98308
  2.9 2.5 %copy-start.2 = (bf16[256,1,2,128]{3,2,1,0:T(2,128)(2,1)S(1)}, bf16[256,1,2,128]{3,2,1,0:T(2,128)(2,1)}, u32[]{:S(2)}) copy-start(bf16[256,1,2,128]{3,2,1,0:T(2,128)(2,1)} %param.23) | copy-start | bytes 393220
  2.9 2.5 %copy-start.3 = (bf16[256,128]{1,0:T(8,128)(2,1)S(1)}, bf16[256,128]{1,0:T(8,128)(2,1)}, u32[]{:S(2)}) copy-start(bf16[256,128]{1,0:T(8,128)(2,1)} %param.21) | copy-start | bytes 196612
  4.5 2.7 %copy-start.4 = (bf16[256,128]{1,0:T(8,128)(2,1)S(1)}, bf16[256,128]{1,0:T(8,128)(2,1)}, u32[]{:S(2)}) copy-start(bf16[256,128]{1,0:T(8,128)(2,1)} %param.20) | copy-start | bytes 196612
  4.5 2.7 %copy-start.7 = (bf16[256,64]{0,1:T(8,128)(2,1)S(1)}, bf16[256,64]{0,1:T(8,128)(2,1)}, u32[]{:S(2)}) copy-start(bf16[256,64]{0,1:T(8,128)(2,1)} %param.17) | copy-start | bytes 98308
  8.3 2.2 %copy-start.11 = (bf16[1,2,128]{2,1,0:T(2,128)(2,1)S(1)}, bf16[1,2,128]{2,1,0:T(2,128)(2,1)}, u32[]{:S(2)}) copy-start(bf16[1,2,128]{2,1,0:T(2,128)(2,1)} %param.25) | copy-start | bytes 1540
  8.3 2.7 %copy-start.8 = (bf16[2048]{0:T(1024)(128)(2,1)S(1)}, bf16[2048]{0:T(1024)(128)(2,1)}, u32[]{:S(2)}) copy-start(bf16[2048]{0:T(1024)(128)(2,1)} %param.27) | copy-start | bytes 12292

commit v2 on v1

--- a/solution.py
+++ b/solution.py
@@ -62,11 +62,10 @@
 
 def kernel(
     n_sp, n_tp, units,
-    w_ref, st_ref, out_ref0, meets_ref, gain_ref, skip_ref, proj_ref, blend_ref, taps_ref,
+    wv_ref, wg_ref, wc_ref, st_ref, out_ref0, meets_ref, gain_ref, skip_ref, proj_ref, blend_ref, taps_ref,
     mixed_ref,
     wbuf, stbuf, acc_state, heads, resid, nb, up, hid, psum, rbuf,
-    own_sem, st_send, st_recv, uz_send, uz_recv, uy_send, uy_recv, cz_send, cz_recv, cy_send,
-    cy_recv, h_send, h_recv, r_send, r_recv, n_send, n_recv, d_send, d_recv,
+    own_sem, st_send, st_recv, z_send, z_recv, y_send, y_recv, h_send, h_recv, r_send, r_recv, n_send, n_recv, d_send, d_recv,
 ):
     s, t = lax.axis_index("sp"), lax.axis_index("tp")
     nz = n_sp // 2
@@ -108,34 +107,40 @@
         def _(o=o):
             st[o].start()
 
-    def zcopies(lo, width, ss, rs):
-        made = []
+    w_refs = (wv_ref, wg_ref, wc_ref)
+    my_rows = pl.ds(pl.multiple_of(q * half, HALO), half)
+    slots = [s] + [lax.rem(z + nz - o, nz) * 2 + y for o in range(1, nz)]
+    side_slots = [slot + 1 - 2 * y for slot in slots]
+    zc, yc = [], []
+    for m in range(3):
+        made = [None]
         for o in range(1, nz):
             zz = lax.rem(z + o, nz)
             rows = pl.ds(pl.multiple_of((zz % 2) * half, HALO), half)
-            made.append(rc(w_ref.at[pl.ds(lo, width), rows], wbuf.at[s, pl.ds(lo, width)],
-                           ss.at[o], rs.at[o], zz * 2 + y, t))
-        return made
-
-    def ycopy(o, lo, width, ss, rs):
-        if o == 0:
-            rows = pl.ds(pl.multiple_of(q * half, HALO), half)
-            source = w_ref.at[pl.ds(lo, width), rows]
-            slot = s
-        else:
-            slot = lax.rem(z + nz - o, nz) * 2 + y
-            source = wbuf.at[slot, pl.ds(lo, width)]
-        return rc(source, wbuf.at[slot, pl.ds(lo, width)], ss.at[o], rs.at[o], side, t)
-
-    uz = zcopies(0, 2, uz_send, uz_recv)
-    uy = [ycopy(o, 0, 2, uy_send, uy_recv) for o in range(nz)]
-    for copy in uz:
+            made.append(rc(w_refs[m].at[rows], wbuf.at[s, m], z_send.at[m, o], z_recv.at[m, o],
+                           zz * 2 + y, t))
+        zc.append(made)
+        yc.append([
+            rc(w_refs[m].at[my_rows] if o == 0 else wbuf.at[slots[o], m], wbuf.at[slots[o], m],
+               y_send.at[m, o], y_recv.at[m, o], side, t)
+            for o in range(nz)
+        ])
+
+    def forward(m, o):
+        zc[m][o].wait_recv()
+        yc[m][o].start()
+
+    for o in range(1, nz):
+        zc[0][o].start()
+        zc[1][o].start()
+    for m in range(3):
+        yc[m][0].start()
+    owns = [
+        pltpu.make_async_copy(w_refs[m].at[my_rows], wbuf.at[s, m], own_sem.at[m])
+        for m in range(3)
+    ]
+    for copy in owns:
         copy.start()
-    uy[0].start()
-    own = pltpu.make_async_copy(
-        w_ref.at[:, pl.ds(pl.multiple_of(q * half, HALO), half)], wbuf.at[s], own_sem
-    )
-    own.start()
 
     acc_state[...] = jnp.zeros_like(acc_state)
     for o in range(n_sp - 1, 0, -1):
@@ -185,6 +190,9 @@
         nb[0, HALO:, piece] = (
             resid[i].astype(F32) * scale * blend_ref[:, piece]
         ).astype(BF16)
+    if nz > 1:
+        forward(0, 1)
+        forward(1, 1)
     after = lax.rem(s + 1, n_sp)
     after_mate = after + 2 - 4 * ((after // 2) % 2)
     block = pl.ds(HALO, tok)
@@ -196,42 +204,63 @@
     ]
     for copy in nc:
         copy.start()
-    cz = zcopies(2, 1, cz_send, cz_recv)
-    cy = [ycopy(o, 2, 1, cy_send, cy_recv) for o in range(nz)]
-    for copy in cz:
-        copy.start()
     for o in range(1, nz):
-        uz[o - 1].wait_recv()
-        uy[o].start()
-    cy[0].start()
-    for copy in nc:
-        copy.wait_recv()
-    own.wait()
-    for o in range(nz):
-        uy[o].wait_recv()
-
+        zc[2][o].start()
     for m in range(2):
         for i in range(2):
             up[m, i] = jnp.zeros_like(up[m, i])
-
-    group = max(1, 128 // dblk)
-
-    def expand_add(b, carry):
-        at = pl.ds(pl.multiple_of(b * group * dblk, 128), group * dblk)
-        for i in range(2):
-            rows = nb[i, :, at]
-            for j in range(group):
-                part = rows[:, j * dblk : (j + 1) * dblk]
+    for copy in nc:
+        copy.wait_recv()
+    for copy in owns:
+        copy.wait()
+    if dblk % 128 == 0:
+
+        def expand(b):
+            at = pl.ds(pl.multiple_of(b * dblk, 128), dblk)
+            for i in range(2):
+                rows = nb[i, :, at]
                 for m in range(2):
                     up[m, i] += lax.dot_general(
-                        part, wbuf[b * group + j, m], NT, preferred_element_type=F32
+                        rows, wbuf[b, m], NT, preferred_element_type=F32
                     )
-        return carry
-
-    lax.fori_loop(0, n_sp // group, expand_add, 0)
-    for o in range(1, nz):
-        cz[o - 1].wait_recv()
-        cy[o].start()
+
+        for o in range(nz):
+            if o > 1:
+                forward(0, o)
+                forward(1, o)
+            expand(slots[o])
+        for o in range(nz):
+            if o == nz - 1:
+                forward(2, 1)
+            yc[0][o].wait_recv()
+            yc[1][o].wait_recv()
+            expand(side_slots[o])
+        for o in range(2, nz):
+            forward(2, o)
+    else:
+        for o in range(2, nz):
+            forward(0, o)
+            forward(1, o)
+        for o in range(nz):
+            yc[0][o].wait_recv()
+            yc[1][o].wait_recv()
+        group = 128 // dblk
+
+        def expand_some(b, carry):
+            at = pl.ds(pl.multiple_of(b * group * dblk, 128), group * dblk)
+            for i in range(2):
+                rows = nb[i, :, at]
+                for j in range(group):
+                    part = rows[:, j * dblk : (j + 1) * dblk]
+                    for m in range(2):
+                        up[m, i] += lax.dot_general(
+                            part, wbuf[b * group + j, m], NT, preferred_element_type=F32
+                        )
+            return carry
+
+        lax.fori_loop(0, n_sp // group, expand_some, 0)
+        for o in range(1, nz):
+            forward(2, o)
     for i in range(2):
         first = (s if i == 0 else mate) == 0
         conv = []
@@ -246,35 +275,80 @@
             conv.append(total)
         value, gate = conv
         hid[pl.ds(i * tok, tok)] = (gate / (1.0 + jnp.exp(-gate)) * value).astype(BF16)
-    for o in range(nz):
-        cy[o].wait_recv()
     per = cols // dblk
-    dc = []
-    for o in range(1, n_tp + 1):
-        to = lax.rem(t + o, n_tp)
+    if dblk % 128 == 0:
+
+        def share(b, i):
+            return rc(psum.at[b, i], rbuf.at[i * n_tp + t, b % per], d_send.at[b, i],
+                      d_recv.at[i * n_tp + t, b % per], s if i == 0 else mate, b // per)
+
+        for k in range(n_sp):
+            b = slots[k] if k < nz else side_slots[k - nz]
+            if k >= nz:
+                yc[2][k - nz].wait_recv()
+            part = jnp.dot(hid[...], wbuf[b, 2], preferred_element_type=F32).astype(BF16)
+            psum[b, 1] = part[tok:]
+            share(b, 1).start()
+            psum[b, 0] = part[:tok]
+
+            @pl.when(b // per != t)
+            def _(b=b):
+                share(b, 0).start()
+
+        sums = []
         for j in range(per):
-            part = jnp.dot(hid[...], wbuf[to * per + j, 2], preferred_element_type=F32).astype(BF16)
-            psum[to, 0, :, j * dblk : (j + 1) * dblk] = part[:tok]
-            psum[to, 1, :, j * dblk : (j + 1) * dblk] = part[tok:]
-        for i in range(2):
-            if i == 0 and o == n_tp:
-                continue
-            at = i * n_tp + o - 1
-            copy = rc(psum.at[to, i], rbuf.at[at], d_send.at[at], d_recv.at[at],
-                      s if i == 0 else mate, to)
-            copy.start()
-            dc.append((at, copy))
-    total = psum[t, 0].astype(F32)
-    for at, copy in dc:
-        copy.wait_recv()
-        total = total + rbuf[at].astype(F32)
-    mixed_ref[...] = (resid[t].astype(F32) + total).astype(BF16)
+            total = resid[t, :, j * dblk : (j + 1) * dblk].astype(F32)
+            total = total + psum[t * per + j, 0].astype(F32)
+            for i in range(2):
+                for o in range(1, n_tp + i):
+                    at = i * n_tp + lax.rem(t + o, n_tp)
+                    rc(psum.at[0, 0], rbuf.at[at, j], d_send.at[0, 0], d_recv.at[at, j],
+                       s if i == 0 else mate, lax.rem(t + o, n_tp) if i == 0 else t).wait_recv()
+                    total = total + rbuf[at, j].astype(F32)
+            sums.append(total.astype(BF16))
+        mixed_ref[...] = jnp.concatenate(sums, axis=1)
+        for k in range(n_sp):
+            b = slots[k] if k < nz else side_slots[k - nz]
+            share(b, 1).wait_send()
+
+            @pl.when(b // per != t)
+            def _(b=b):
+                share(b, 0).wait_send()
+        dc = []
+    else:
+        for o in range(nz):
+            yc[2][o].wait_recv()
+        dc = []
+        for o in range(1, n_tp + 1):
+            to = lax.rem(t + o, n_tp)
+            for j in range(per):
+                part = jnp.dot(
+                    hid[...], wbuf[to * per + j, 2], preferred_element_type=F32
+                ).astype(BF16)
+                psum[to, 0, :, j * dblk : (j + 1) * dblk] = part[:tok]
+                psum[to, 1, :, j * dblk : (j + 1) * dblk] = part[tok:]
+            for i in range(2):
+                if i == 0 and o == n_tp:
+                    continue
+                at = i * n_tp + o - 1
+                copy = rc(psum.at[to, i], rbuf.at[at], d_send.at[at, 0], d_recv.at[at, 0],
+                          s if i == 0 else mate, to)
+                copy.start()
+                dc.append((at, copy))
+        total = psum[t, 0].astype(F32)
+        for at, copy in dc:
+            copy.wait_recv()
+            total = total + rbuf[at].astype(F32)
+        mixed_ref[...] = (resid[t].astype(F32) + total).astype(BF16)
 
     for o in range(1, n_sp):
         @pl.when(s + o < n_sp)
         def _(o=o):
             st[o].wait_send()
-    for copy in uz + uy + cz + cy + hc + qc + nc + [c for _, c in dc]:
+    for m in range(3):
+        for copy in zc[m][1:] + yc[m]:
+            copy.wait_send()
+    for copy in hc + qc + nc + [c for _, c in dc]:
         copy.wait_send()
 
 
@@ -329,9 +403,6 @@
         ],
         axis=0,
     ).astype(BF16)
-    weights = jnp.stack(
-        [content_expansion_matrix.T, switch_expansion_matrix.T, contraction_matrix], axis=0
-    )
     ff = contraction_matrix.shape[0]
     half = ff // 2
     dblk = contraction_matrix.shape[1]
@@ -343,11 +414,24 @@
     nz = n_sp // 2
     model = n_tp * cols
     dma = pltpu.SemaphoreType.DMA
+    per = cols // dblk
+    if dblk % 128 == 0:
+        shares = (
+            pltpu.VMEM((n_sp, 2, tok, dblk), BF16),
+            pltpu.VMEM((2 * n_tp, per, tok, dblk), BF16),
+        )
+        sent, got = (n_sp, 2), (2 * n_tp, per)
+    else:
+        shares = (
+            pltpu.VMEM((n_tp, 2, tok, cols), BF16),
+            pltpu.VMEM((2 * n_tp, tok, cols), BF16),
+        )
+        sent, got = (2 * n_tp, 1), (2 * n_tp, 1)
     vmem = pl.BlockSpec(memory_space=pltpu.VMEM)
     return pl.pallas_call(
         functools.partial(kernel, n_sp, n_tp, units),
         out_shape=jax.ShapeDtypeStruct((tok, cols), BF16),
-        in_specs=[vmem] * 9,
+        in_specs=[vmem] * 11,
         out_specs=vmem,
         scratch_shapes=[
             pltpu.VMEM((n_sp, 3, half, dblk), BF16),
@@ -358,19 +442,17 @@
             pltpu.VMEM((2, tok + HALO, model), BF16),
             pltpu.VMEM((2, 2, tok + HALO, half), F32),
             pltpu.VMEM((2 * tok, half), BF16),
-            pltpu.VMEM((n_tp, 2, tok, cols), BF16),
-            pltpu.VMEM((2 * n_tp, tok, cols), BF16),
-            dma,
+            *shares,
+            dma((3,)),
             dma((n_sp,)), dma((n_sp,)),
-            dma((nz,)), dma((nz,)), dma((nz,)), dma((nz,)),
-            dma((nz,)), dma((nz,)), dma((nz,)), dma((nz,)),
+            dma((3, nz)), dma((3, nz)), dma((3, nz)), dma((3, nz)),
             dma((n_tp,)), dma((n_tp,)), dma((n_tp,)), dma((n_tp,)),
-            dma((3,)), dma((3,)), dma((2 * n_tp,)), dma((2 * n_tp,)),
+            dma((3,)), dma((3,)), dma(sent), dma(got),
         ],
         compiler_params=pltpu.CompilerParams(
             collective_id=0, has_side_effects=True, vmem_limit_bytes=56 * 1024 * 1024
         ),
-    )(weights, packed, out, meets, gain, skip_stream, final_projection_matrix, blend, taps)
+    )(content_expansion_matrix.T, switch_expansion_matrix.T, contraction_matrix, packed, out, meets, gain, skip_stream, final_projection_matrix, blend, taps)
 
 
 def solution(mesh):

time: 184 us -> 203 us (1.10)
  Pallas kernels: 170 us -> 185 us
  local copies, waits for them, and re-layouts: 6.56 us -> 11.4 us
    pallas_call x1, Pallas kernels: 170 us -> 185 us  [local(): pl.pallas_call(functools.partial(kernel, n_sp, n_tp, units), out_shape=ja...]
    unnamed x31 -> x33, local copies, waits for them, and re-layouts: 4.89 us -> 9.77 us
where the time goes in v2:
time: 203 us
  Pallas kernels  185 us (91%)
  local copies, waits for them, and re-layouts  11.4 us (6%)
  other arithmetic  3.04 us (1%)
  matrix products  2.54 us (1%)
    pallas_call x1, Pallas kernels, local(): pl.pallas_call(functools.partial(kernel, n_sp, n_tp, units), out_shape=ja...  185 us
    unnamed x33, local copies, waits for them, and re-layouts  9.77 us

profile of v2, /device:TPU:16, one launch (start us, length us, event | category | flops | bytes accessed | tf_op | source)
XLA Modules:
  0.0 202.7 jit_solution(10134291299859231250)
XLA Ops:
  0.1 0.6 copy-done.12
  0.7 0.6 bitcast_convert_fusion.gain_ref
  1.4 0.6 copy-done.9
  2.0 0.6 reshape.120
  2.7 0.6 pad_convert_fusion.taps_ref
  3.6 0.7 copy-done.7
  4.5 0.7 copy-done.8
  5.4 0.8 copy-done.5
  6.2 0.8 copy-done.11
  7.0 0.4 fusion.14
  7.6 0.7 copy-done.4
  8.3 0.6 convolution_select_fusion
  8.9 0.3 copy-done.3
  9.2 0.3 fusion.28
  9.5 0.2 copy.40
  9.7 0.6 convolution_bitcast_fusion
  10.7 0.6 fusion
  11.4 0.2 copy.39
  11.7 0.8 copy_bitcast_fusion
  12.5 0.7 maximum_maximum_fusion.st_ref
  13.3 1.2 copy.31
  14.4 1.2 copy.30
  15.6 185.4 %shard_map.154 = bf16[256,512]{1,0:T(8,128)(2,1)} custom-call(bf16[1408,256]{1,0:T(8,128)(2,1)} %bitcast.122, bf16[1408,256]{1,0:T(8,128)(2,1)} %bitcast.121, bf16[1408,256]{1,0:T(8,128)(2,1)} %wc_ref.1, bf16[144,256]{1,0:T(8,128)(2,1)} %maximum_maximum_fusion.st_ref, f32[256,256]{1,0:T(8,128)} %get-tuple-element.16.out_ref0, ...), custom_call_target="tpu_custom_call" | custom-call | tf_op jit(solution)/shard_map/pallas_call | solution.py:431
  201.0 1.7 copy.65
  (44 shorter events, 1.5 us)
Async XLA Ops:
  0.0 2.6 %copy-start = (bf16[3,2,1408]{2,1,0:T(2,128)(2,1)S(1)}, bf16[3,2,1408]{2,1,0:T(2,128)(2,1)}, u32[]{:S(2)}) copy-start(bf16[3,2,1408]{2,1,0:T(2,128)(2,1)} %param.30) | copy-start | bytes 50692
  0.0 0.7 copy-start.12
  0.1 1.2 copy-start.10
  1.3 0.7 copy-start.9
  2.7 0.8 copy-start.6
  3.6 0.8 copy-start.7
  4.4 0.8 copy-start.8
  5.3 0.8 copy-start.5
  6.2 0.8 copy-start.11
  7.5 0.8 copy-start.4
  8.3 0.9 copy-start.3
  11.6 1.7 copy-start.1
  13.3 1.2 copy-start.2
